TPU v7x, 32 devices: a whole 2x2x4 slice. The times are simulated.
32 devices in a mesh: grp: 2 (over y), sp: 4 (over z), tp: 4 (over x, core).
Axes of the slice: x: 2, y: 2, z: 4, core: 2. Of those that a mesh axis runs over, the one named last changes fastest.
Arguments:
- queries: bfloat16 [4096, 1024], P(('grp', 'sp'), 'tp'), parts along dimension 0, may hold values from -6 to 6
- memory_keys: bfloat16 [4096, 1024], P(('grp', 'sp'), 'tp'), parts along dimension 0, may hold values from -6 to 6
- memory_values: bfloat16 [4096, 1024], P(('grp', 'sp'), 'tp'), parts along dimension 0, may hold values from -6 to 6
- output_preactivation: bfloat16 [4096, 1024], P(('grp', 'sp'), 'tp'), parts along dimension 0, may hold values from -12 to 12
- input_preactivation: float32 [8, 4096], P('tp', ('grp', 'sp')), parts along dimension 1, may hold values from -6 to 140
- forget_preactivation: float32 [8, 4096], P('tp', ('grp', 'sp')), parts along dimension 1, as said below
- extra_forget_terms: float32 [8, 4096], P('tp', ('grp', 'sp')), parts along dimension 1, may hold values from -1 to 0, as said below
- head_norm_gain: float32 [128], replicated, may hold values from 0.1 to 1.9
- output_projection_matrix: bfloat16 [1024, 2048], P('tp'), may hold values from -0.1875 to 0.1875
- residual: bfloat16 [4096, 2048], P(('grp', 'sp', 'tp')), parts along dimension 0, may hold values from -6 to 6
- feedforward_norm_gain: float32 [2048], replicated, may hold values from 0.1 to 1.9
- feedforward_up_matrix: bfloat16 [2048, 8192], P('sp', 'tp'), may hold values from -0.125 to 0.125
- feedforward_down_matrix: bfloat16 [8192, 2048], P('tp', 'sp'), may hold values from -0.0625 to 0.0625
Outputs:
- layer_out: bfloat16 [4096, 2048], P(('grp', 'sp', 'tp')), parts along dimension 0
There are 2 independent parts, one for each index of `grp`. A program takes and returns all parts, laid end to end along the dimension named above; an argument that names none is the same for every part. Nothing has to cross between parts.
Inputs may be any that keep to these rules, and one draw needn't show every extreme that they name: `forget_preactivation`: forget gate pre-activations. `extra_forget_terms`: extra log forget terms, zero at most positions.
All inputs are finite; a program needn't handle non-finite values.
Results may differ from a plain program's by a relative error of at most 0.018.
Values may be sent and summed in bfloat16 or wider, within the bound.
A program may use at most 64 MiB of HBM per device.

v0:
```python
import jax
import jax.numpy as jnp
from jax import lax
from jax.sharding import PartitionSpec as P

BLOCK = 128
neg_big = -1e30
norm_eps = 1e-06
highest = lax.Precision.HIGHEST


def entering(x, axis, combine, identity):
    length, position = (lax.axis_size(axis), lax.axis_index(axis))
    everything = jax.tree.map(lambda part: lax.all_gather(part, axis), x)
    start = jax.tree.map(
        lambda part, zero: jnp.broadcast_to(jnp.asarray(zero, part.dtype), part.shape), x, identity
    )

    def step(k, before):
        reached = k < position
        new = combine(before, jax.tree.map(lambda part: part[k], everything))
        return jax.tree.map(lambda a, b: jnp.where(reached, a, b), new, before)

    return lax.fori_loop(0, length, step, start)


def rms_norm(tensor, gain_vec):
    mean_sq = jnp.mean(tensor * tensor, axis=-1, keepdims=True)
    return tensor * lax.rsqrt(mean_sq + norm_eps) * gain_vec


def combine(earlier, later):
    total_e, max_e, memory_e = earlier
    total_l, max_l, memory_l = later
    carried = total_l + max_e
    new_max = jnp.maximum(carried, max_l)
    old_part = jnp.exp(carried - new_max)
    new_part = jnp.exp(max_l - new_max)
    return (
        total_e + total_l,
        new_max,
        old_part[..., None, None] * memory_e + new_part[..., None, None] * memory_l,
    )


def block_summary(key_blk, val_blk, gate_blk, decay_logarithm):
    block_total = decay_logarithm[..., -1]
    tail_log = block_total[..., None] - decay_logarithm + gate_blk
    tail_max = jnp.max(tail_log, axis=-1)
    weights = jnp.exp(tail_log - tail_max[..., None])
    memory = jnp.einsum("bhsv,bhsk->bhvk", weights[..., None] * val_blk, key_blk, precision=highest)
    return (block_total, tail_max, memory)


def shards(
    queries,
    memory_keys,
    memory_values,
    output_preactivation,
    input_preactivation,
    forget_preactivation,
    extra_forget_terms,
    head_norm_gain,
    output_projection_matrix,
    residual,
    feedforward_norm_gain,
    feedforward_up_matrix,
    feedforward_down_matrix,
):
    tok_count = queries.shape[0]
    head_count = input_preactivation.shape[0]
    head_dim = queries.shape[1] // head_count
    block_len = BLOCK
    block_count = tok_count // block_len

    def to_blocks(tensor):
        return (
            tensor.astype(jnp.float32)
            .reshape(block_count, block_len, head_count, head_dim)
            .transpose(0, 2, 1, 3)
        )

    def gate_block_list(tensor):
        return tensor.reshape(head_count, block_count, block_len).transpose(1, 0, 2)

    query_blk = to_blocks(queries)
    key_blk = to_blocks(memory_keys) * head_dim ** (-0.5)
    val_blk = to_blocks(memory_values)
    gate_blk = gate_block_list(input_preactivation)
    decay_logarithm = jnp.cumsum(
        gate_block_list(jax.nn.log_sigmoid(forget_preactivation) + extra_forget_terms), axis=-1
    )
    summaries = block_summary(key_blk, val_blk, gate_blk, decay_logarithm)
    zero_heads = jnp.zeros((head_count,), jnp.float32)
    zero_memory = jnp.zeros((head_count, head_dim, head_dim), jnp.float32)
    zero_state = (zero_heads, jnp.full((head_count,), neg_big, jnp.float32), zero_memory)
    prefixes = []
    running = zero_state
    for block_idx in range(block_count):
        prefixes.append(running)
        running = combine(running, tuple((member[block_idx] for member in summaries)))
    before = entering(running, "sp", combine, zero_state)
    anchor = (zero_heads, zero_heads, zero_memory)
    incoming = combine(anchor, before)
    starts = [combine(incoming, prefix) for prefix in prefixes]
    start_max = jnp.stack([each_state[1] for each_state in starts])
    start_memory = jnp.stack([each_state[2] for each_state in starts])
    causal = lax.broadcasted_iota(jnp.int32, (block_len, block_len), 0) >= lax.broadcasted_iota(
        jnp.int32, (block_len, block_len), 1
    )
    log_weight = (
        decay_logarithm[..., :, None] - decay_logarithm[..., None, :] + gate_blk[..., None, :]
    )
    log_weight = jnp.where(causal, log_weight, neg_big)
    carry_log = decay_logarithm + start_max[..., None]
    row_max = jnp.maximum(jnp.max(log_weight, axis=-1), carry_log)
    scores = jnp.einsum("bhtd,bhsd->bhts", query_blk, key_blk, precision=highest) * jnp.exp(
        log_weight - row_max[..., None]
    )
    carry_scale = jnp.exp(carry_log - row_max)
    hidden = jnp.einsum("bhts,bhsv->bhtv", scores, val_blk, precision=highest)
    hidden = hidden + carry_scale[..., None] * jnp.einsum(
        "bhvk,bhtk->bhtv", start_memory, query_blk, precision=highest
    )
    hidden = hidden.transpose(0, 2, 1, 3).reshape(tok_count, head_count, head_dim)
    gated = rms_norm(hidden, head_norm_gain) * jax.nn.sigmoid(
        output_preactivation.astype(jnp.float32).reshape(tok_count, head_count, head_dim)
    )
    mixed = gated.reshape(tok_count, head_count * head_dim).astype(jnp.bfloat16)
    branch = lax.psum_scatter(
        jnp.dot(mixed, output_projection_matrix, preferred_element_type=jnp.float32).astype(
            jnp.bfloat16
        ),
        "tp",
        scatter_dimension=0,
        tiled=True,
    ).astype(jnp.float32)
    mid_state = (residual.astype(jnp.float32) + branch).astype(jnp.bfloat16)
    normed = rms_norm(mid_state.astype(jnp.float32), feedforward_norm_gain).astype(jnp.bfloat16)
    normed_all = lax.all_gather(normed, "tp", axis=0, tiled=True)
    upward = jnp.dot(
        normed_all,
        lax.all_gather(feedforward_up_matrix, "sp", axis=0, tiled=True),
        preferred_element_type=jnp.float32,
    )
    active = jnp.square(jax.nn.relu(upward)).astype(jnp.bfloat16)
    mlp_terms = jnp.dot(
        active,
        lax.all_gather(feedforward_down_matrix, "sp", axis=1, tiled=True),
        preferred_element_type=jnp.float32,
    )
    mlp_sum = lax.psum_scatter(
        mlp_terms.astype(jnp.bfloat16), "tp", scatter_dimension=0, tiled=True
    ).astype(jnp.float32)
    return (mid_state.astype(jnp.float32) + mlp_sum).astype(jnp.bfloat16)


def solution(mesh):
    in_specs = (
        P(("grp", "sp"), "tp"),
        P(("grp", "sp"), "tp"),
        P(("grp", "sp"), "tp"),
        P(("grp", "sp"), "tp"),
        P("tp", ("grp", "sp")),
        P("tp", ("grp", "sp")),
        P("tp", ("grp", "sp")),
        P(),
        P("tp", None),
        P(("grp", "sp", "tp"), None),
        P(),
        P("sp", "tp"),
        P("tp", "sp"),
    )
    out_specs = P(("grp", "sp", "tp"), None)
    return jax.shard_map(shards, mesh=mesh, in_specs=in_specs, out_specs=out_specs, check_vma=False)
```

profile of v0, /device:TPU:0, one launch (start us, length us, event | category | flops | bytes accessed | tf_op | source)
XLA Modules:
  0.0 468.9 jit_solution(10719103995341335332)
XLA Ops:
  6.6 0.8 fusion.50
  7.4 1.2 reduce_window_sum.11
  9.1 0.9 fusion.65
  10.0 0.8 subtract_exponential_fusion.2
  10.8 12.6 %all-gather.1 = f32[4,1,2]{2,1,0:T(1,128)S(1)} all-gather(f32[1,1,2]{2,1,0:T(1,128)S(1)} %get-tuple-element.255), channel_id=1, replica_groups=mesh['grp'=2,'sp'=4,'tp'=4] {'sp'}, dimensions={0}, use_global_device_ids=true | all-gather | bytes 40 | tf_op jit(solution)/shard_map/all_gather | solution.py:14
  23.5 7.6 %all-gather = f32[4,1,2]{2,1,0:T(1,128)S(1)} all-gather(f32[1,1,2]{2,1,0:T(1,128)S(1)} %get-tuple-element.256), channel_id=1, replica_groups=mesh['grp'=2,'sp'=4,'tp'=4] {'sp'}, dimensions={0}, use_global_device_ids=true | all-gather | bytes 40 | tf_op jit(solution)/shard_map/all_gather | solution.py:14
  31.0 1.0 reshape.306
  32.2 1.0 convert_multiply_fusion.2
  33.5 0.7 fusion.22
  34.4 15.0 %all_gather.23 = f32[4,2,128,128]{3,2,1,0:T(8,128)S(1)} all-gather(f32[1,2,128,128]{3,2,1,0:T(8,128)S(1)} %fusion.40), channel_id=1, replica_groups=mesh['grp'=2,'sp'=4,'tp'=4] {'sp'}, dimensions={0}, use_global_device_ids=true | all-gather | bytes 655360 | tf_op jit(solution)/shard_map/all_gather | solution.py:14
  49.4 0.6 while.18
  50.7 0.7 fusion.5
  51.7 0.7 fusion.7
  53.9 2.1 convolution_convert_fusion
  56.1 31.6 %reduce-scatter.3.cloned.1.call-done = bf16[128,2048]{1,0:T(8,128)(2,1)} async-done(((bf16[512,2048]{1,0:T(8,128)(2,1)}), bf16[128,2048]{1,0:T(8,128)(2,1)}) %reduce-scatter.3.cloned.1.call-update) | async-done | bytes 524304 | tf_op jit(solution)/shard_map/reduce_scatter | solution.py:130
  87.6 1.3 fusion.8
  89.0 2.0 fusion.10
  91.1 0.7 all-gather.8.cloned.1.call-update
  92.6 21.2 %all-gather.6.cloned.1.call-done = bf16[512,2048]{1,0:T(8,128)(2,1)} async-done(((bf16[128,2048]{1,0:T(8,128)(2,1)}), bf16[512,2048]{1,0:T(8,128)(2,1)}) %all-gather.6.cloned.1.call-update) | async-done | bytes 2097168 | tf_op jit(solution)/shard_map/all_gather | solution.py:140
  113.8 151.2 %all-gather.8.cloned.1.call-done = bf16[2048,2048]{1,0:T(8,128)(2,1)} async-done(((bf16[512,2048]{1,0:T(8,128)(2,1)}), bf16[2048,2048]{1,0:T(8,128)(2,1)}) %all-gather.8.cloned.1.call-update) | async-done | bytes 8388624 | tf_op jit(solution)/shard_map/all_gather | solution.py:143
  265.0 149.3 %all-gather.10.cloned.1.call-done = bf16[2048,2048]{1,0:T(8,128)(2,1)} async-done(((bf16[2048,512]{1,0:T(8,128)(2,1)}), bf16[2048,2048]{1,0:T(8,128)(2,1)}) %all-gather.10.cloned.1.call-update) | async-done | bytes 8388624 | tf_op jit(solution)/shard_map/all_gather | solution.py:149
  414.2 16.5 %convolution_convert_fusion.1 = bf16[512,2048]{1,0:T(8,128)(2,1)} fusion(bf16[2048,2048]{1,0:T(8,128)(2,1)} %all-gather.10.cloned.1.call-done, bf16[512,2048]{1,0:T(8,128)(2,1)} %all-gather.6.cloned.1.call-done, bf16[2048,2048]{1,0:T(8,128)(2,1)} %all-gather.8.cloned.1.call-done), kind=kOutput, calls=%fused_computation.16 | convolution fusion | flops 8594128896 | bytes 20971520 | tf_op jit(solution)/shard_map/dot_general | solution.py:147
  430.8 29.5 %reduce-scatter.5.cloned.1.call-done = bf16[128,2048]{1,0:T(8,128)(2,1)} async-done(((bf16[512,2048]{1,0:T(8,128)(2,1)}), bf16[128,2048]{1,0:T(8,128)(2,1)}) %reduce-scatter.5.cloned.1.call-update) | async-done | bytes 524304 | tf_op jit(solution)/shard_map/reduce_scatter | solution.py:152
  460.3 2.1 fusion.11
  (68 shorter events, 5.0 us)
Async XLA Ops:
  6.5 47.3 %copy-start = (bf16[256,2048]{1,0:T(8,128)(2,1)S(1)}, bf16[256,2048]{1,0:T(8,128)(2,1)}, u32[]{:S(2)}) copy-start(bf16[256,2048]{1,0:T(8,128)(2,1)} %param.23) | copy-start | bytes 3145732
  6.5 43.5 %copy-start.4 = (f32[2,512]{1,0:T(2,128)S(1)}, f32[2,512]{1,0:T(2,128)}, u32[]{:S(2)}) copy-start(f32[2,512]{1,0:T(2,128)} %param.19) | copy-start | bytes 12292
  6.5 44.1 %copy-start.7 = (f32[128]{0:T(128)S(1)}, f32[128]{0:T(128)}, u32[]{:S(2)}) copy-start(f32[128]{0:T(128)} %param.22) | copy-start | bytes 1540
  6.5 44.1 %copy-start.3 = (bf16[512,256]{1,0:T(8,128)(2,1)S(1)}, bf16[512,256]{1,0:T(8,128)(2,1)}, u32[]{:S(2)}) copy-start(bf16[512,256]{1,0:T(8,128)(2,1)} %param.15) | copy-start | bytes 786436
  6.5 81.1 %reduce-scatter.3.cloned.1.call-start = ((), (), s32[]{:S(2)}) async-start(), calls=%async_computation.2 | async-start | bytes 2621440 | tf_op jit(solution)/shard_map/reduce_scatter | solution.py:130
  50.7 3.2 copy-start.6
  53.0 34.7 %copy-start.1 = (bf16[128,2048]{1,0:T(8,128)(2,1)S(1)}, bf16[128,2048]{1,0:T(8,128)(2,1)}, u32[]{:S(2)}) copy-start(bf16[128,2048]{1,0:T(8,128)(2,1)} %param.24) | copy-start | bytes 1572868
  53.9 35.1 %copy-start.5 = (f32[2048]{0:T(1024)S(1)}, f32[2048]{0:T(1024)}, u32[]{:S(2)}) copy-start(f32[2048]{0:T(1024)} %param.25) | copy-start | bytes 24580
  56.0 57.7 %all-gather.6.cloned.1.call-start = ((), (), s32[]{:S(2)}) async-start(), calls=%async_computation.3 | async-start | bytes 2621440 | tf_op jit(solution)/shard_map/all_gather | solution.py:140
  91.0 174.0 %all-gather.8.cloned.1.call-start = ((), (), s32[]{:S(2)}) async-start(), calls=%async_computation.4 | async-start | bytes 10485760 | tf_op jit(solution)/shard_map/all_gather | solution.py:143
  91.8 322.5 %all-gather.10.cloned.1.call-start = ((), (), s32[]{:S(2)}) async-start(), calls=%async_computation.5 | async-start | bytes 10485760 | tf_op jit(solution)/shard_map/all_gather | solution.py:149
  92.3 368.0 %copy-start.2 = (bf16[128,2048]{1,0:T(8,128)(2,1)S(1)}, bf16[128,2048]{1,0:T(8,128)(2,1)}, u32[]{:S(2)}) copy-start(bf16[128,2048]{1,0:T(8,128)(2,1)} %reduce-scatter.3.cloned.1.call-done) | copy-start | bytes 1572868
  92.3 367.9 %reduce-scatter.5.cloned.1.call-start = ((), (), s32[]{:S(2)}) async-start(), calls=%async_computation.6 | async-start | bytes 2621440 | tf_op jit(solution)/shard_map/reduce_scatter | solution.py:152
Sparse Core Ops, SparseCore 0:
  56.1 31.4 reduce-scatter.2
  91.1 22.5 all-gather.5
  115.3 149.6 all-gather.7
  266.4 147.7 all-gather.9
  430.9 29.3 reduce-scatter.4
where the time goes:
time: 469 us
  waiting for transfers between devices  384 us (82%)
  blocking collectives  35.2 us (8%)
  matrix products  21.1 us (4%)
  between operations  13.4 us (3%)
  other arithmetic  11.6 us (2%)
    all_gather x1, waiting for transfers between devices, shards(): lax.all_gather(feedforward_up_matrix, 'sp', axis=0, tiled=True)  151 us
    all_gather x1, waiting for transfers between devices, shards(): lax.all_gather(feedforward_down_matrix, 'sp', axis=1, tiled=True)  149 us
    all_gather x3, blocking collectives, entering(): everything = jax.tree.map(lambda part: lax.all_gather(part, axis), x)  35.2 us
    reduce_scatter x1, waiting for transfers between devices, shards(): lax.psum_scatter(jnp.dot(mixed, output_projection_matrix, preferred_eleme...  31.6 us
    reduce_scatter x1, waiting for transfers between devices, shards(): lax.psum_scatter(mlp_terms.astype(jnp.bfloat16), 'tp', scatter_dimension=...  29.5 us
    all_gather x1, waiting for transfers between devices, shards(): normed_all = lax.all_gather(normed, 'tp', axis=0, tiled=True)  21.2 us
    dot_general x1, matrix products, shards(): jnp.dot(active, lax.all_gather(feedforward_down_matrix, 'sp', axis=1, til...  16.5 us
  transfers between devices with their start and end apart: 5, of which 5 were waited for; matrix products, arithmetic and copies ran while one was open for 0% of the time, Pallas kernels for 0%

commit v1 on v0

--- a/solution.py
+++ b/solution.py
@@ -146,7 +146,7 @@
     active = jnp.square(jax.nn.relu(upward)).astype(jnp.bfloat16)
     mlp_terms = jnp.dot(
         active,
-        lax.all_gather(feedforward_down_matrix, "sp", axis=1, tiled=True),
+        jnp.concatenate(lax.all_gather(feedforward_down_matrix, "sp"), axis=1),
         preferred_element_type=jnp.float32,
     )
     mlp_sum = lax.psum_scatter(

time: 469 us -> 439 us (0.936)
  waiting for transfers between devices: 384 us -> 338 us
  local copies, waits for them, and re-layouts: 3.07 us -> 14.7 us
    all_gather x1, waiting for transfers between devices: 149 us -> 116 us  [shards(): lax.all_gather(feedforward_down_matrix, 'sp')]
    reshape x0 -> x1, local copies, waits for them, and re-layouts: none -> 11.6 us  [shards(): jnp.concatenate(lax.all_gather(feedforward_down_matrix, 'sp'), axis=1)]
    all_gather x1, waiting for transfers between devices: 21.2 us -> 10.5 us  [shards(): normed_all = lax.all_gather(normed, 'tp', axis=0, tiled=True)]
  transfers between devices with their start and end apart: 5 -> 5, of which waited for: 5 -> 5; matrix products, arithmetic and copies ran while one was open for 0% -> 3% of each run, Pallas kernels for 0% -> 0%
where the time goes in v1:
time: 439 us; the launch traced here: 438 us
  waiting for transfers between devices  338 us (77%)
  blocking collectives  36.6 us (8%)
  matrix products  21.2 us (5%)
  between operations  15.3 us (3%)
  local copies, waits for them, and re-layouts  14.7 us (3%)
  other arithmetic  11.6 us (3%)
    all_gather x1, waiting for transfers between devices, shards(): lax.all_gather(feedforward_up_matrix, 'sp', axis=0, tiled=True)  151 us
    all_gather x1, waiting for transfers between devices, shards(): lax.all_gather(feedforward_down_matrix, 'sp')  116 us
    all_gather x3, blocking collectives, entering(): everything = jax.tree.map(lambda part: lax.all_gather(part, axis), x)  36.6 us
    reduce_scatter x1, waiting for transfers between devices, shards(): lax.psum_scatter(jnp.dot(mixed, output_projection_matrix, preferred_eleme...  30.3 us
    reduce_scatter x1, waiting for transfers between devices, shards(): lax.psum_scatter(mlp_terms.astype(jnp.bfloat16), 'tp', scatter_dimension=...  29.5 us
    dot_general x1, matrix products, shards(): jnp.dot(active, jnp.concatenate(lax.all_gather(feedforward_down_matrix, '...  16.6 us
    reshape x1, local copies, waits for them, and re-layouts, shards(): jnp.concatenate(lax.all_gather(feedforward_down_matrix, 'sp'), axis=1)  11.6 us
    all_gather x1, waiting for transfers between devices, shards(): normed_all = lax.all_gather(normed, 'tp', axis=0, tiled=True)  10.5 us
  transfers between devices with their start and end apart: 5, of which 5 were waited for; matrix products, arithmetic and copies ran while one was open for 3% of the time, Pallas kernels for 0%

profile of v1, /device:TPU:0, one launch (start us, length us, event | category | flops | bytes accessed | tf_op | source)
XLA Modules:
  0.0 438.3 jit_solution(4009372981847480919)
XLA Ops:
  7.4 0.8 fusion.50
  8.2 1.2 reduce_window_sum.11
  9.9 0.8 fusion.65
  10.8 0.8 subtract_exponential_fusion.2
  11.6 1.0 convert_multiply_fusion.2
  12.9 1.0 reshape.312
  14.1 0.7 fusion.22
  15.0 17.4 %all_gather.26 = f32[4,2,128,128]{3,2,1,0:T(8,128)S(1)} all-gather(f32[1,2,128,128]{3,2,1,0:T(8,128)S(1)} %fusion.40), channel_id=1, replica_groups=mesh['grp'=2,'sp'=4,'tp'=4] {'sp'}, dimensions={0}, use_global_device_ids=true | all-gather | bytes 655360 | tf_op jit(solution)/shard_map/all_gather | solution.py:14
  32.3 11.7 %all-gather.2 = f32[4,1,2]{2,1,0:T(1,128)S(1)} all-gather(f32[1,1,2]{2,1,0:T(1,128)S(1)} %get-tuple-element.263), channel_id=1, replica_groups=mesh['grp'=2,'sp'=4,'tp'=4] {'sp'}, dimensions={0}, use_global_device_ids=true | all-gather | bytes 40 | tf_op jit(solution)/shard_map/all_gather | solution.py:14
  44.0 7.6 %all-gather.1 = f32[4,1,2]{2,1,0:T(1,128)S(1)} all-gather(f32[1,1,2]{2,1,0:T(1,128)S(1)} %get-tuple-element.264), channel_id=1, replica_groups=mesh['grp'=2,'sp'=4,'tp'=4] {'sp'}, dimensions={0}, use_global_device_ids=true | all-gather | bytes 40 | tf_op jit(solution)/shard_map/all_gather | solution.py:14
  51.6 0.6 while.18
  52.9 0.7 fusion.5
  53.9 0.7 fusion.7
  56.1 2.1 convolution_convert_fusion
  58.9 30.3 %reduce-scatter.3.cloned.1.call-done = bf16[128,2048]{1,0:T(8,128)(2,1)} async-done(((bf16[512,2048]{1,0:T(8,128)(2,1)}), bf16[128,2048]{1,0:T(8,128)(2,1)}) %reduce-scatter.3.cloned.1.call-update) | async-done | bytes 524304 | tf_op jit(solution)/shard_map/reduce_scatter | solution.py:130
  89.2 1.3 fusion.8
  90.5 2.0 fusion.10
  93.4 116.1 %all-gather.11.cloned.1.call-done = bf16[8192,512]{1,0:T(8,128)(2,1)} async-done(((bf16[2048,512]{1,0:T(8,128)(2,1)}), bf16[8192,512]{1,0:T(8,128)(2,1)}) %all-gather.11.cloned.1.call-update) | async-done | bytes 8388624 | tf_op jit(solution)/shard_map/all_gather | solution.py:149
  209.4 11.6 %copy.74 = bf16[2048,4,512]{0,2,1:T(8,128)(2,1)} copy(bf16[2048,4,512]{2,0,1:T(8,128)(2,1)} %bitcast.210) | data formatting | bytes 16777216 | tf_op jit(solution)/shard_map/reshape | solution.py:149
  221.0 10.5 %all-gather.7.cloned.1.call-done = bf16[512,2048]{1,0:T(8,128)(2,1)} async-done(((bf16[128,2048]{1,0:T(8,128)(2,1)}), bf16[512,2048]{1,0:T(8,128)(2,1)}) %all-gather.7.cloned.1.call-update) | async-done | bytes 2097168 | tf_op jit(solution)/shard_map/all_gather | solution.py:140
  231.5 150.9 %all-gather.9.cloned.1.call-done = bf16[2048,2048]{1,0:T(8,128)(2,1)} async-done(((bf16[512,2048]{1,0:T(8,128)(2,1)}), bf16[2048,2048]{1,0:T(8,128)(2,1)}) %all-gather.9.cloned.1.call-update) | async-done | bytes 8388624 | tf_op jit(solution)/shard_map/all_gather | solution.py:143
  382.5 16.6 %convolution_convert_fusion.1 = bf16[512,2048]{1,0:T(8,128)(2,1)} fusion(bf16[2048,2048]{0,1:T(8,128)(2,1)} %bitcast.211, bf16[512,2048]{1,0:T(8,128)(2,1)} %all-gather.7.cloned.1.call-done, bf16[2048,2048]{1,0:T(8,128)(2,1)} %all-gather.9.cloned.1.call-done), kind=kOutput, calls=%fused_computation.16 | convolution fusion | flops 8594128896 | bytes 20971520 | tf_op jit(solution)/shard_map/dot_general | solution.py:147
  399.1 29.5 %reduce-scatter.5.cloned.1.call-done = bf16[128,2048]{1,0:T(8,128)(2,1)} async-done(((bf16[512,2048]{1,0:T(8,128)(2,1)}), bf16[128,2048]{1,0:T(8,128)(2,1)}) %reduce-scatter.5.cloned.1.call-update) | async-done | bytes 524304 | tf_op jit(solution)/shard_map/reduce_scatter | solution.py:152
  428.6 2.1 fusion.11
  (69 shorter events, 5.5 us)
Async XLA Ops:
  7.4 48.7 %copy-start = (bf16[256,2048]{1,0:T(8,128)(2,1)S(1)}, bf16[256,2048]{1,0:T(8,128)(2,1)}, u32[]{:S(2)}) copy-start(bf16[256,2048]{1,0:T(8,128)(2,1)} %param.23) | copy-start | bytes 3145732
  7.4 44.9 %copy-start.4 = (f32[2,512]{1,0:T(2,128)S(1)}, f32[2,512]{1,0:T(2,128)}, u32[]{:S(2)}) copy-start(f32[2,512]{1,0:T(2,128)} %param.19) | copy-start | bytes 12292
  7.4 45.4 %copy-start.3 = (bf16[512,256]{1,0:T(8,128)(2,1)S(1)}, bf16[512,256]{1,0:T(8,128)(2,1)}, u32[]{:S(2)}) copy-start(bf16[512,256]{1,0:T(8,128)(2,1)} %param.15) | copy-start | bytes 786436
  7.4 81.8 %reduce-scatter.3.cloned.1.call-start = ((), (), s32[]{:S(2)}) async-start(), calls=%async_computation.2 | async-start | bytes 2621440 | tf_op jit(solution)/shard_map/reduce_scatter | solution.py:130
  52.2 3.2 copy-start.7
  52.9 3.2 copy-start.6
  56.1 33.1 %copy-start.1 = (bf16[128,2048]{1,0:T(8,128)(2,1)S(1)}, bf16[128,2048]{1,0:T(8,128)(2,1)}, u32[]{:S(2)}) copy-start(bf16[128,2048]{1,0:T(8,128)(2,1)} %param.24) | copy-start | bytes 1572868
  56.1 34.4 %copy-start.5 = (f32[2048]{0:T(1024)S(1)}, f32[2048]{0:T(1024)}, u32[]{:S(2)}) copy-start(f32[2048]{0:T(1024)} %param.25) | copy-start | bytes 24580
  58.2 151.2 %all-gather.11.cloned.1.call-start = ((), (), s32[]{:S(2)}) async-start(), calls=%async_computation.6 | async-start | bytes 10485760 | tf_op jit(solution)/shard_map/all_gather | solution.py:149
  58.8 172.7 %all-gather.7.cloned.1.call-start = ((), (), s32[]{:S(2)}) async-start(), calls=%async_computation.3 | async-start | bytes 2621440 | tf_op jit(solution)/shard_map/all_gather | solution.py:140
  92.6 289.9 %all-gather.9.cloned.1.call-start = ((), (), s32[]{:S(2)}) async-start(), calls=%async_computation.4 | async-start | bytes 10485760 | tf_op jit(solution)/shard_map/all_gather | solution.py:143
  93.2 335.4 %reduce-scatter.5.cloned.1.call-start = ((), (), s32[]{:S(2)}) async-start(), calls=%async_computation.5 | async-start | bytes 2621440 | tf_op jit(solution)/shard_map/reduce_scatter | solution.py:152
  382.5 46.1 %copy-start.2 = (bf16[128,2048]{1,0:T(8,128)(2,1)S(1)}, bf16[128,2048]{1,0:T(8,128)(2,1)}, u32[]{:S(2)}) copy-start(bf16[128,2048]{1,0:T(8,128)(2,1)} %reduce-scatter.3.cloned.1.call-done) | copy-start | bytes 1572868
Sparse Core Ops, SparseCore 0:
  58.3 30.8 reduce-scatter.2
  399.2 29.3 reduce-scatter.4
Sparse Core Ops, SparseCore 1:
  60.3 149.1 all-gather.10
  210.9 20.6 all-gather.6
  233.0 149.5 all-gather.8
